TPU v7x, 512 devices: a 8x2x16 block of a 8x8x16 slice. The times are simulated.
512 devices in a mesh: grp: 2 (over y), dp: 8 (over x), kv: 16 (over z), tp: 2 (over core).
Axes of the slice: x: 8, y: 2, z: 16, core: 2. Of those that a mesh axis runs over, the one named last changes fastest.
The devices are a block of a 8x8x16 slice.
Arguments:
- inputs: bfloat16 [512, 4096], P(('grp', 'dp'), 'kv'), parts along dimension 0, may hold values from -6 to 6
- gain_in: float32 [4096], P('kv'), may hold values from 0.1 to 1.9
- w_gate: bfloat16 [4096, 2048], P('kv', 'tp'), may hold values from -0.09375 to 0.09375
- w_input: bfloat16 [4096, 2048], P('kv', 'tp'), may hold values from -0.09375 to 0.09375
- w_bproj: bfloat16 [4096, 1024], P('kv', 'tp'), may hold values from -0.09375 to 0.09375
- w_cproj: bfloat16 [4096, 1024], P('kv', 'tp'), may hold values from -0.09375 to 0.09375
- w_step: bfloat16 [4096, 32], P('kv', 'tp'), may hold values from -0.09375 to 0.09375
- conv_input: float32 [4, 2048], P(None, 'tp'), may hold values from -3 to 3
- conv_bproj: float32 [4, 1024], P(None, 'tp'), may hold values from -3 to 3
- conv_cproj: float32 [4, 1024], P(None, 'tp'), may hold values from -3 to 3
- tail_input: bfloat16 [512, 3, 2048], P(('grp', 'dp', 'kv'), None, 'tp'), parts along dimension 0, may hold values from -6 to 6
- tail_bproj: bfloat16 [512, 3, 1024], P(('grp', 'dp', 'kv'), None, 'tp'), parts along dimension 0, may hold values from -6 to 6
- tail_cproj: bfloat16 [512, 3, 1024], P(('grp', 'dp', 'kv'), None, 'tp'), parts along dimension 0, may hold values from -6 to 6
- step_bias: float32 [32], P('tp'), may hold values from -3 to 0
- decay_log: float32 [32], P('tp'), may hold values from -2 to 2
- block_input: bfloat16 [512, 128, 2048], P(('grp', 'dp', 'kv'), None, 'tp'), parts along dimension 0, may hold values from -6 to 6
- block_bproj: bfloat16 [512, 128, 1024], P(('grp', 'dp', 'kv'), None, 'tp'), parts along dimension 0, may hold values from -0.59765625 to 0.59765625
- block_step: float32 [512, 128, 32], P(('grp', 'dp', 'kv'), None, 'tp'), parts along dimension 0, may hold values from 0.005 to 0.2
- lengths: int32 [512], P(('grp', 'dp', 'kv')), parts along dimension 0, may hold values from 1 to 127, 8192 in all
- state: float32 [512, 32, 64, 128], P(('grp', 'dp', 'kv'), 'tp'), parts along dimension 0, may hold values from -0.6 to 0.6
- gain_mix: float32 [2048], P('tp'), may hold values from 0.1 to 1.9
- w_out: bfloat16 [2048, 4096], P('tp', 'kv'), may hold values from -0.125 to 0.125
- gain_mlp: float32 [4096], P(('kv', 'tp')), may hold values from 0.1 to 1.9
- w_up: bfloat16 [4096, 16384], P(('kv', 'tp'), 'dp'), may hold values from -0.09375 to 0.09375
- w_down: bfloat16 [16384, 4096], P('dp', ('kv', 'tp')), may hold values from -0.046875 to 0.046875
Outputs:
- layer_out: bfloat16 [512, 4096], P(('grp', 'dp'), ('kv', 'tp')), parts along dimension 0
There are 2 independent parts, one for each index of `grp`. A program takes and returns all parts, laid end to end along the dimension named above; an argument that names none is the same for every part. Nothing has to cross between parts.
Inputs may be any that keep to these rules, and one draw needn't show every extreme that they name: `lengths`: the number of live positions before the new token in each sequence's current block; the largest equals 127 in every draw.
All inputs are finite; a program needn't handle non-finite values.
Results may differ from a plain program's by a relative error of at most 0.012.
Values may be sent and summed in bfloat16 or wider, within the bound.
No kernel may reach another device: no remote copies, remote signals or barrier semaphores. Data moves between devices by JAX's collectives and lax.ppermute only.
A program may use at most 64 MiB of HBM per device.

v0:
```python
import jax
import jax.numpy as jnp
from jax import lax
from jax.sharding import PartitionSpec as P

D = 4096
HEAD_DIM = 64
D_STATE = 128
TAPS = 4
SSM_WIDTH = 2048
LANES = 128
EPS = 1e-06
BF16 = jnp.bfloat16
F32 = jnp.float32


def two_words(x):
    high = lax.reduce_precision(x, 8, 7)
    return (high.astype(BF16), (x - high).astype(BF16))


def to_everyone(shard, axes):
    size = lax.axis_size(axes)
    return lax.all_to_all(
        jnp.broadcast_to(shard[None], (size, *shard.shape)), axes, 0, 0, tiled=True
    )


def from_partner(x):
    size = lax.axis_size("tp")
    return lax.ppermute(x, "tp", [(i, (i + 1) % size) for i in range(size)])


def exchanged(weight, dim, core):
    half = weight.shape[dim] // 2
    mine = lax.dynamic_slice_in_dim(weight, core * half, half, dim)
    other = lax.dynamic_slice_in_dim(weight, (1 - core) * half, half, dim)
    return (mine, from_partner(other))


def in_core_order(mine, other, core, dim):
    return jnp.where(
        core == 0,
        jnp.concatenate([mine, other], axis=dim),
        jnp.concatenate([other, mine], axis=dim),
    )


def convolve(history, weights, newest):
    summed = weights[TAPS - 1] * newest
    for offset in range(TAPS - 1):
        summed = summed + weights[offset] * history[:, offset].astype(F32)
    return jax.nn.silu(summed)


def per_device(
    inputs,
    gain_in,
    w_gate,
    w_input,
    w_bproj,
    w_cproj,
    w_step,
    conv_input,
    conv_bproj,
    conv_cproj,
    tail_input,
    tail_bproj,
    tail_cproj,
    step_bias,
    decay_log,
    block_input,
    block_bproj,
    block_step,
    lengths,
    state,
    gain_mix,
    w_out,
    gain_mlp,
    w_up,
    w_down,
):
    core = lax.axis_index("tp")
    n_kv, n_dp, n_tp = (lax.axis_size("kv"), lax.axis_size("dp"), lax.axis_size("tp"))
    stream = inputs.astype(F32)
    rows = inputs.shape[0]
    squares = jnp.sum(stream * stream, axis=1)
    scaled = (stream * gain_in).astype(BF16)
    matrices = (w_gate, w_input, w_bproj, w_cproj)
    pieces = [
        jnp.dot(scaled, weight, preferred_element_type=F32).astype(BF16) for weight in matrices
    ]
    pieces += two_words(jnp.dot(scaled, w_step, preferred_element_type=F32))
    pieces += two_words(squares[:, None])
    bounds = [0]
    for piece in pieces:
        bounds.append(bounds[-1] + piece.shape[1])
    spare = -bounds[-1] % LANES
    pieces.append(jnp.zeros((rows, spare), BF16))
    sent = jnp.concatenate(pieces, axis=1).reshape(n_kv, rows // n_kv, -1)
    arrived = lax.all_to_all(sent, "kv", 0, 0, tiled=True)
    projected = jnp.sum(arrived.astype(F32), axis=0)
    out_mine, out_other = exchanged(w_out, 1, core)
    up_mine, up_other = exchanged(w_up, 1, core)
    down_mine, down_other = exchanged(w_down, 0, core)
    gain_other = from_partner(gain_mlp)
    out_weight = jnp.concatenate([out_mine, out_other], axis=0)
    up_weight = jnp.concatenate([up_mine, up_other], axis=0)
    down_weight = in_core_order(down_mine, down_other, core, 1)
    up_gain = jnp.concatenate([gain_mlp, gain_other])
    parts = [projected[:, a:b] for a, b in zip(bounds[:-1], bounds[1:])]
    inverse = lax.rsqrt((parts[6] + parts[7]) / D + EPS)
    gate_pre, value_pre, b_pre, c_pre = [parts[k] * inverse for k in range(4)]
    step_pre = (parts[4] + parts[5]) * inverse
    seq_count = lengths.shape[0]
    head_count = step_bias.shape[0]
    group_count = w_bproj.shape[1] // D_STATE
    block_len = block_step.shape[1]
    per_group = head_count // group_count
    current = convolve(tail_input, conv_input, value_pre)
    b_now = convolve(tail_bproj, conv_bproj, b_pre)
    c_now = convolve(tail_cproj, conv_cproj, c_pre)
    step_size = jax.nn.softplus(step_pre + step_bias)
    decay_rate = -jnp.exp(decay_log)
    positions = lax.broadcasted_iota(jnp.int32, (1, block_len), 1)
    live_rows = (positions < lengths[:, None]).astype(F32)
    masked = block_step * live_rows[:, :, None]
    later_steps = jnp.sum(masked, axis=1, keepdims=True) - jnp.cumsum(masked, axis=1)
    decays = jnp.exp(decay_rate * (step_size[:, None, :] + later_steps)) * live_rows[:, :, None]
    c_query = c_now.astype(BF16).reshape(seq_count, group_count, D_STATE)
    keys = block_bproj.reshape(seq_count, block_len, group_count, D_STATE)
    scores = jnp.einsum("bsgn,bgn->bsg", keys, c_query, preferred_element_type=F32)
    scores = jnp.repeat(scores, per_group, axis=2)
    weights = (decays * scores * block_step).astype(BF16)
    values = block_input.reshape(seq_count, block_len, head_count, HEAD_DIM)
    inner_sum = jnp.einsum("bsh,bshp->bhp", weights, values, preferred_element_type=F32)
    c_full = c_now.reshape(seq_count, group_count, D_STATE)
    b_full = b_now.reshape(seq_count, group_count, D_STATE)
    own_score = jnp.repeat(jnp.sum(c_full * b_full, axis=2), per_group, axis=1)
    own_term = (step_size * own_score)[:, :, None] * current.reshape(
        seq_count, head_count, HEAD_DIM
    )
    carried = jnp.exp(decay_rate * (step_size + jnp.sum(masked, axis=1)))
    c_heads = jnp.repeat(c_full, per_group, axis=1)
    readout = jnp.einsum("bhpn,bhn->bhp", state, c_heads, precision=lax.Precision.HIGHEST)
    mixed = (inner_sum + own_term + carried[:, :, None] * readout).reshape(
        seq_count, -1
    ) * jax.nn.silu(gate_pre)
    width = mixed.shape[1]
    local_sq = two_words(jnp.sum(mixed * mixed, axis=1, keepdims=True))
    row = jnp.concatenate(
        [(mixed * gain_mix).astype(BF16), *local_sq, jnp.zeros((seq_count, LANES - 2), BF16)],
        axis=1,
    )
    whole = to_everyone(row, ("kv", "tp")).reshape(n_kv, n_tp, seq_count, -1)
    whole = jnp.moveaxis(whole, 1, 0).reshape(n_tp, rows, -1)
    total_sq = jnp.sum(whole[:, :, width : width + 2].astype(F32), axis=(0, 2))
    halves = whole[:, :, :width]
    channels = jnp.concatenate(
        [
            lax.dynamic_index_in_dim(halves, core, 0, keepdims=False),
            lax.dynamic_index_in_dim(halves, 1 - core, 0, keepdims=False),
        ],
        axis=1,
    )
    mixed_in = jnp.dot(channels, out_weight, preferred_element_type=F32)
    mixed_in = mixed_in * lax.rsqrt(total_sq / SSM_WIDTH + EPS)[:, None]
    column_count = mixed_in.shape[1]
    residual = lax.dynamic_slice_in_dim(stream, core * column_count, column_count, 1)
    hidden = (residual + mixed_in).astype(BF16)
    all_hidden = to_everyone(hidden, ("dp", "tp")).reshape(n_dp, n_tp, rows, -1)
    all_hidden = jnp.moveaxis(all_hidden, 1, 0).reshape(n_tp, n_dp * rows, -1)
    all_hidden = jnp.concatenate(
        [
            lax.dynamic_index_in_dim(all_hidden, core, 0, keepdims=False),
            lax.dynamic_index_in_dim(all_hidden, 1 - core, 0, keepdims=False),
        ],
        axis=1,
    ).astype(F32)
    row_sq = jnp.sum(all_hidden * all_hidden, axis=1)
    lifted = (all_hidden * up_gain).astype(BF16)
    raised = lax.dot_general(
        up_weight, lifted, (((0,), (1,)), ((), ())), preferred_element_type=F32
    ).astype(BF16)
    seqs = raised.shape[1]
    extra = jnp.concatenate(
        [*[w[None] for w in two_words(row_sq)], jnp.zeros((6, seqs), BF16)], axis=0
    )
    sent = jnp.concatenate(
        [raised.reshape(n_kv, -1, seqs), jnp.broadcast_to(extra[None], (n_kv, *extra.shape))],
        axis=1,
    )
    arrived = lax.all_to_all(sent, "kv", 0, 0, tiled=True)
    shares = jnp.sum(arrived.astype(F32), axis=0)
    unit_count = shares.shape[0] - 8
    sq_sum = shares[unit_count] + shares[unit_count + 1]
    units = jnp.square(
        jax.nn.relu(shares[:unit_count] * lax.rsqrt(sq_sum / D + EPS)[None, :])
    ).astype(BF16)
    hidden_units = lax.all_gather(units, "kv", axis=0, tiled=True)
    lowered = lax.dot_general(
        hidden_units, down_weight, (((0,), (0,)), ((), ())), preferred_element_type=F32
    ).astype(BF16)
    lowered = lowered.reshape(n_dp, rows, n_tp, -1)
    lowered = jnp.moveaxis(lowered, 2, 1).reshape(n_dp * n_tp, rows, -1)
    lowered = lax.all_to_all(lowered, ("dp", "tp"), 0, 0, tiled=True)
    return (hidden.astype(F32) + jnp.sum(lowered.astype(F32), axis=0)).astype(BF16)


def solution(mesh):
    return jax.shard_map(
        per_device,
        mesh=mesh,
        in_specs=(
            P(("grp", "dp"), "kv"),
            P("kv"),
            P("kv", "tp"),
            P("kv", "tp"),
            P("kv", "tp"),
            P("kv", "tp"),
            P("kv", "tp"),
            P(None, "tp"),
            P(None, "tp"),
            P(None, "tp"),
            P(("grp", "dp", "kv"), None, "tp"),
            P(("grp", "dp", "kv"), None, "tp"),
            P(("grp", "dp", "kv"), None, "tp"),
            P("tp"),
            P("tp"),
            P(("grp", "dp", "kv"), None, "tp"),
            P(("grp", "dp", "kv"), None, "tp"),
            P(("grp", "dp", "kv"), None, "tp"),
            P(("grp", "dp", "kv")),
            P(("grp", "dp", "kv"), "tp", None, None),
            P("tp"),
            P("tp", "kv"),
            P(("kv", "tp")),
            P(("kv", "tp"), "dp"),
            P("dp", ("kv", "tp")),
        ),
        out_specs=P(("grp", "dp"), ("kv", "tp")),
        check_vma=False,
    )
```

profile of v0, /device:TPU:65, one launch (start us, length us, event | category | flops | bytes accessed | tf_op | source)
XLA Modules:
  0.0 200.1 jit_solution(6419792693657834448)
XLA Ops:
  0.0 0.9 multiply_reduce_fusion
  1.4 0.9 fusion.26
  2.4 1.1 convolution_convert_fusion.5
  3.6 1.1 convolution_convert_fusion.4
  4.8 1.3 convolution_convert_fusion.3
  6.4 1.1 concatenate.52
  7.5 44.2 %all-to-all-start = ((bf16[16,2,3200]{2,1,0:T(2,128)(2,1)}), bf16[16,2,3200]{2,1,0:T(2,128)(2,1)S(1)}, u32[]{:S(2)}, u32[]{:S(2)}) async-start(bf16[16,2,3200]{2,1,0:T(2,128)(2,1)} %concatenate.52), calls=%async_computation | async-start | bytes 409600 | tf_op jit(solution)/shard_map/all_to_all | solution.py:101
  52.9 11.0 %all-to-all-done = bf16[16,2,3200]{2,1,0:T(2,128)(2,1)S(1)} async-done(((bf16[16,2,3200]{2,1,0:T(2,128)(2,1)}), bf16[16,2,3200]{2,1,0:T(2,128)(2,1)S(1)}, u32[]{:S(2)}, u32[]{:S(2)}) %all-to-all-start) | async-done | bytes 204832 | tf_op jit(solution)/shard_map/all_to_all | solution.py:101
  65.5 1.7 fusion.62
  68.3 0.8 broadcast_in_dim.23
  69.0 10.6 %all-to-all-start.1 = ((bf16[32,2,1152]{2,1,0:T(2,128)(2,1)}), bf16[32,2,1152]{2,1,0:T(2,128)(2,1)S(1)}, u32[]{:S(2)}, u32[]{:S(2)}) async-start(bf16[32,2,1152]{2,1,0:T(2,128)(2,1)} %broadcast_in_dim.23), calls=%async_computation.1 | async-start | bytes 294912 | tf_op jit(solution)/shard_map/all_to_all | solution.py:24
  79.7 2.6 %collective-permute-start = (bf16[1024,128]{1,0:T(8,128)(2,1)S(1)}, bf16[1024,128]{1,0:T(8,128)(2,1)S(1)}, u32[]{:S(2)}, u32[]{:S(2)}) collective-permute-start(bf16[1024,128]{1,0:T(8,128)(2,1)S(1)} %get-tuple-element.18), channel_id=1, source_target_pairs={{0,1},{1,0},{2,3},{3,2},{4,5},{5,4},{6,7},{7,6},{8,9},{9,8},{10,11... | collective-permute-start | bytes 786440 | tf_op jit(solution)/shard_map/ppermute | solution.py:31
  82.3 13.6 %all-to-all-done.1 = bf16[32,2,1152]{2,1,0:T(2,128)(2,1)S(1)} async-done(((bf16[32,2,1152]{2,1,0:T(2,128)(2,1)}), bf16[32,2,1152]{2,1,0:T(2,128)(2,1)S(1)}, u32[]{:S(2)}, u32[]{:S(2)}) %all-to-all-start.1) | async-done | bytes 147488 | tf_op jit(solution)/shard_map/all_to_all | solution.py:24
  97.1 0.7 broadcast_in_dim.24
  97.7 8.9 %all-to-all-start.2 = ((bf16[16,32,128]{2,1,0:T(8,128)(2,1)}), bf16[16,32,128]{2,1,0:T(8,128)(2,1)S(1)}, u32[]{:S(2)}, u32[]{:S(2)}) async-start(bf16[16,32,128]{2,1,0:T(8,128)(2,1)} %broadcast_in_dim.24), calls=%async_computation.2 | async-start | bytes 262144 | tf_op jit(solution)/shard_map/all_to_all | solution.py:24
  106.6 2.2 %collective-permute-start.2 = (f32[128]{0:T(128)S(1)}, f32[128]{0:T(128)S(1)}, u32[]{:S(2)}, u32[]{:S(2)}) collective-permute-start(f32[128]{0:T(128)S(1)} %copy-done.18), channel_id=1, source_target_pairs={{0,1},{1,0},{2,3},{3,2},{4,5},{5,4},{6,7},{7,6},{8,9},{9,8},{10,11... | collective-permute-start | bytes 1544 | tf_op jit(solution)/shard_map/ppermute | solution.py:31
  109.0 2.1 %collective-permute-start.1 = (bf16[128,1024]{1,0:T(8,128)(2,1)S(1)}, bf16[128,1024]{1,0:T(8,128)(2,1)S(1)}, u32[]{:S(2)}, u32[]{:S(2)}) collective-permute-start(bf16[128,1024]{1,0:T(8,128)(2,1)S(1)} %get-tuple-element.16), channel_id=1, source_target_pairs={{0,1},{1,0},{2,3},{3,2},{4,5},{5,4},{6,7},{7,6},{8,9},{9,8},{10,11... | collective-permute-start | bytes 786440 | tf_op jit(solution)/shard_map/ppermute | solution.py:31
  111.2 4.3 %all-to-all-done.2 = bf16[16,32,128]{2,1,0:T(8,128)(2,1)S(1)} async-done(((bf16[16,32,128]{2,1,0:T(8,128)(2,1)}), bf16[16,32,128]{2,1,0:T(8,128)(2,1)S(1)}, u32[]{:S(2)}, u32[]{:S(2)}) %all-to-all-start.2) | async-done | bytes 131104 | tf_op jit(solution)/shard_map/all_to_all | solution.py:24
  116.2 0.9 pad_maximum_fusion
  117.0 4.0 %all-to-all-start.3 = ((bf16[16,72,256]{2,1,0:T(8,128)(2,1)}), bf16[16,72,256]{2,1,0:T(8,128)(2,1)S(1)}, u32[]{:S(2)}, u32[]{:S(2)}) async-start(bf16[16,72,256]{2,1,0:T(8,128)(2,1)} %pad_maximum_fusion), calls=%async_computation.3 | async-start | bytes 1179648 | tf_op jit(solution)/shard_map/all_to_all | solution.py:193
  121.1 2.0 collective-permute-start.3
  123.1 26.3 %all-to-all-done.3 = bf16[16,72,256]{2,1,0:T(8,128)(2,1)S(1)} async-done(((bf16[16,72,256]{2,1,0:T(8,128)(2,1)}), bf16[16,72,256]{2,1,0:T(8,128)(2,1)S(1)}, u32[]{:S(2)}, u32[]{:S(2)}) %all-to-all-start.3) | async-done | bytes 589856 | tf_op jit(solution)/shard_map/all_to_all | solution.py:193
  149.5 27.8 %all_gather.3 = bf16[1024,256]{1,0:T(8,128)(2,1)S(1)} all-gather(bf16[64,256]{1,0:T(8,128)(2,1)S(1)} %fusion.24), channel_id=1, replica_groups=mesh['grp'=2,'dp'=8,'kv'=16,'tp'=2] {'kv'}, dimensions={0}, use_global_device_ids=true | all-gather | bytes 557056 | tf_op jit(solution)/shard_map/all_gather | solution.py:200
  177.7 21.7 %all_to_all.25 = bf16[16,32,128]{2,1,0:T(8,128)(2,1)S(1)} all-to-all(bf16[16,32,128]{2,1,0:T(8,128)(2,1)S(1)} %bitcast.105), channel_id=1, replica_groups=mesh['grp'=2,'dp'=8,'kv'=16,'tp'=2] {'dp','tp'}, dimensions={0} | all-to-all | bytes 262144 | tf_op jit(solution)/shard_map/all_to_all | solution.py:206
  (126 shorter events, 7.5 us)
Async XLA Ops:
  0.0 65.5 %copy-start = (f32[2,16,64,128]{3,2,1,0:T(8,128)S(1)}, f32[2,16,64,128]{3,2,1,0:T(8,128)}, u32[]{:S(2)}) copy-start(f32[2,16,64,128]{3,2,1,0:T(8,128)} %param.44) | copy-start | bytes 3145732
  0.0 6.1 %copy-start.1 = (bf16[32,256]{1,0:T(8,128)(2,1)S(1)}, bf16[32,256]{1,0:T(8,128)(2,1)}, u32[]{:S(2)}) copy-start(bf16[32,256]{1,0:T(8,128)(2,1)} %param.25) | copy-start | bytes 49156
  0.0 6.1 %copy-start.8 = (f32[256]{0:T(256)S(1)}, f32[256]{0:T(256)}, u32[]{:S(2)}) copy-start(f32[256]{0:T(256)} %param.26) | copy-start | bytes 3076
  0.0 6.1 %copy-start.5 = (bf16[256,1024]{1,0:T(8,128)(2,1)S(1)}, bf16[256,1024]{1,0:T(8,128)(2,1)}, u32[]{:S(2)}) copy-start(bf16[256,1024]{1,0:T(8,128)(2,1)} %param.28) | copy-start | bytes 1572868
  4.7 47.0 %copy-start.19 = (s32[2]{0:T(128)S(1)}, s32[2]{0:T(128)}, u32[]{:S(2)}) copy-start(s32[2]{0:T(128)} %param.43) | copy-start | bytes 28
  4.8 47.1 %copy-start.9 = (f32[2,128,16]{1,2,0:T(8,128)S(1)}, f32[2,128,16]{1,2,0:T(8,128)}, u32[]{:S(2)}) copy-start(f32[2,128,16]{1,2,0:T(8,128)} %param.42) | copy-start | bytes 49156
  6.0 46.0 %copy-start.20 = (f32[16]{0:T(128)S(1)}, f32[16]{0:T(128)}, u32[]{:S(2)}) copy-start(f32[16]{0:T(128)} %param.39) | copy-start | bytes 196
  6.1 46.0 %copy-start.7 = (bf16[2,128,512]{2,1,0:T(8,128)(2,1)S(1)}, bf16[2,128,512]{2,1,0:T(8,128)(2,1)}, u32[]{:S(2)}) copy-start(bf16[2,128,512]{2,1,0:T(8,128)(2,1)} %param.41) | copy-start | bytes 786436
  6.3 46.0 %copy-start.6 = (bf16[2,128,1024]{2,1,0:T(8,128)(2,1)S(1)}, bf16[2,128,1024]{2,1,0:T(8,128)(2,1)}, u32[]{:S(2)}) copy-start(bf16[2,128,1024]{2,1,0:T(8,128)(2,1)} %param.40) | copy-start | bytes 1572868
  7.5 56.4 %all-to-all-start = ((bf16[16,2,3200]{2,1,0:T(2,128)(2,1)}), bf16[16,2,3200]{2,1,0:T(2,128)(2,1)S(1)}, u32[]{:S(2)}, u32[]{:S(2)}) async-start(bf16[16,2,3200]{2,1,0:T(2,128)(2,1)} %concatenate.52), calls=%async_computation | async-start | bytes 409600 | tf_op jit(solution)/shard_map/all_to_all | solution.py:101
  52.1 12.2 %copy-start.14 = (bf16[2,3,512]{2,0,1:T(2,128)(2,1)S(1)}, bf16[2,3,512]{2,0,1:T(2,128)(2,1)}, u32[]{:S(2)}) copy-start(bf16[2,3,512]{2,0,1:T(2,128)(2,1)} %param.37) | copy-start | bytes 18436
  52.1 12.2 %copy-start.15 = (bf16[2,3,512]{2,0,1:T(2,128)(2,1)S(1)}, bf16[2,3,512]{2,0,1:T(2,128)(2,1)}, u32[]{:S(2)}) copy-start(bf16[2,3,512]{2,0,1:T(2,128)(2,1)} %param.36) | copy-start | bytes 18436
  52.1 12.6 %copy-start.11 = (bf16[2,3,1024]{2,0,1:T(2,128)(2,1)S(1)}, bf16[2,3,1024]{2,0,1:T(2,128)(2,1)}, u32[]{:S(2)}) copy-start(bf16[2,3,1024]{2,0,1:T(2,128)(2,1)} %param.35) | copy-start | bytes 36868
  52.3 12.8 %copy-start.17 = (f32[16]{0:T(128)S(1)}, f32[16]{0:T(128)}, u32[]{:S(2)}) copy-start(f32[16]{0:T(128)} %param.38) | copy-start | bytes 196
  65.5 14.1 %copy-start.2 = (bf16[1024,256]{1,0:T(8,128)(2,1)S(1)}, bf16[1024,256]{1,0:T(8,128)(2,1)}, u32[]{:S(2)}) copy-start(bf16[1024,256]{1,0:T(8,128)(2,1)} %param.46) | copy-start | bytes 1572868
  69.0 26.9 %all-to-all-start.1 = ((bf16[32,2,1152]{2,1,0:T(2,128)(2,1)}), bf16[32,2,1152]{2,1,0:T(2,128)(2,1)S(1)}, u32[]{:S(2)}, u32[]{:S(2)}) async-start(bf16[32,2,1152]{2,1,0:T(2,128)(2,1)} %broadcast_in_dim.23), calls=%async_computation.1 | async-start | bytes 294912 | tf_op jit(solution)/shard_map/all_to_all | solution.py:24
  79.7 17.2 %collective-permute-start = (bf16[1024,128]{1,0:T(8,128)(2,1)S(1)}, bf16[1024,128]{1,0:T(8,128)(2,1)S(1)}, u32[]{:S(2)}, u32[]{:S(2)}) collective-permute-start(bf16[1024,128]{1,0:T(8,128)(2,1)S(1)} %get-tuple-element.18), channel_id=1, source_target_pairs={{0,1},{1,0},{2,3},{3,2},{4,5},{5,4},{6,7},{7,6},{8,9},{9,8},{10,11... | collective-permute-start | bytes 786440 | tf_op jit(solution)/shard_map/ppermute | solution.py:31
  96.7 9.9 %copy-start.18 = (f32[128]{0:T(128)S(1)}, f32[128]{0:T(128)}, u32[]{:S(2)}) copy-start(f32[128]{0:T(128)} %param.47) | copy-start | bytes 1540
  96.8 12.1 %copy-start.3 = (bf16[128,2048]{1,0:T(8,128)(2,1)S(1)}, bf16[128,2048]{1,0:T(8,128)(2,1)}, u32[]{:S(2)}) copy-start(bf16[128,2048]{1,0:T(8,128)(2,1)} %param.48) | copy-start | bytes 1572868
  97.7 17.8 %all-to-all-start.2 = ((bf16[16,32,128]{2,1,0:T(8,128)(2,1)}), bf16[16,32,128]{2,1,0:T(8,128)(2,1)S(1)}, u32[]{:S(2)}, u32[]{:S(2)}) async-start(bf16[16,32,128]{2,1,0:T(8,128)(2,1)} %broadcast_in_dim.24), calls=%async_computation.2 | async-start | bytes 262144 | tf_op jit(solution)/shard_map/all_to_all | solution.py:24
  106.6 4.6 %collective-permute-start.2 = (f32[128]{0:T(128)S(1)}, f32[128]{0:T(128)S(1)}, u32[]{:S(2)}, u32[]{:S(2)}) collective-permute-start(f32[128]{0:T(128)S(1)} %copy-done.18), channel_id=1, source_target_pairs={{0,1},{1,0},{2,3},{3,2},{4,5},{5,4},{6,7},{7,6},{8,9},{9,8},{10,11... | collective-permute-start | bytes 1544 | tf_op jit(solution)/shard_map/ppermute | solution.py:31
  109.0 6.8 %collective-permute-start.1 = (bf16[128,1024]{1,0:T(8,128)(2,1)S(1)}, bf16[128,1024]{1,0:T(8,128)(2,1)S(1)}, u32[]{:S(2)}, u32[]{:S(2)}) collective-permute-start(bf16[128,1024]{1,0:T(8,128)(2,1)S(1)} %get-tuple-element.16), channel_id=1, source_target_pairs={{0,1},{1,0},{2,3},{3,2},{4,5},{5,4},{6,7},{7,6},{8,9},{9,8},{10,11... | collective-permute-start | bytes 786440 | tf_op jit(solution)/shard_map/ppermute | solution.py:31
  117.0 32.4 %all-to-all-start.3 = ((bf16[16,72,256]{2,1,0:T(8,128)(2,1)}), bf16[16,72,256]{2,1,0:T(8,128)(2,1)S(1)}, u32[]{:S(2)}, u32[]{:S(2)}) async-start(bf16[16,72,256]{2,1,0:T(8,128)(2,1)} %pad_maximum_fusion), calls=%async_computation.3 | async-start | bytes 1179648 | tf_op jit(solution)/shard_map/all_to_all | solution.py:193
  121.1 56.2 %collective-permute-start.3 = (bf16[1024,128]{1,0:T(8,128)(2,1)S(1)}, bf16[1024,128]{1,0:T(8,128)(2,1)S(1)}, u32[]{:S(2)}, u32[]{:S(2)}) collective-permute-start(bf16[1024,128]{1,0:T(8,128)(2,1)S(1)} %get-tuple-element.14), channel_id=1, source_target_pairs={{0,1},{1,0},{2,3},{3,2},{4,5},{5,4},{6,7},{7,6},{8,9},{9,8},{10,11... | collective-permute-start | bytes 786440 | tf_op jit(solution)/shard_map/ppermute | solution.py:31
  (5 other events, 10.3 us)
where the time goes:
time: 201 us; the launch traced here: 200 us
  starting transfers between devices  76.7 us (38%)
  waiting for transfers between devices  55.3 us (28%)
  blocking collectives  49.5 us (25%)
  matrix products  7.82 us (4%)
  local copies, waits for them, and re-layouts  5.53 us (3%)
  other arithmetic  4.62 us (2%)
    all_to_all x2, starting transfers between devices, per_device(): arrived = lax.all_to_all(sent, 'kv', 0, 0, tiled=True)  48.2 us
    all_to_all x2, waiting for transfers between devices, per_device(): arrived = lax.all_to_all(sent, 'kv', 0, 0, tiled=True)  37.3 us
    all_gather x1, blocking collectives, per_device(): hidden_units = lax.all_gather(units, 'kv', axis=0, tiled=True)  27.8 us
    all_to_all x1, blocking collectives, per_device(): lowered = lax.all_to_all(lowered, ('dp', 'tp'), 0, 0, tiled=True)  21.7 us
    all_to_all x2, starting transfers between devices, to_everyone(): lax.all_to_all(jnp.broadcast_to(shard[None], (size, *shard.shape)), axes,...  19.5 us
    all_to_all x2, waiting for transfers between devices, to_everyone(): lax.all_to_all(jnp.broadcast_to(shard[None], (size, *shard.shape)), axes,...  17.9 us
    ppermute x4, starting transfers between devices, from_partner(): return lax.ppermute(x, 'tp', [(i, (i + 1) % size) for i in range(size)])  8.98 us
  transfers between devices with their start and end apart: 8, of which 4 were waited for; matrix products, arithmetic and copies ran while one was open for 1% of the time, Pallas kernels for 0%

commit v1 on v0

--- a/solution.py
+++ b/solution.py
@@ -12,6 +12,19 @@
 EPS = 1e-06
 BF16 = jnp.bfloat16
 F32 = jnp.float32
+
+
+def collect(x, axis, dim):
+    ways = lax.axis_size(axis)
+    up = [(d, (d + 1) % ways) for d in range(ways)]
+    down = [(d, (d - 1) % ways) for d in range(ways)]
+    earlier, later = ([x], [x])
+    for _ in range(ways // 2):
+        earlier.append(lax.ppermute(earlier[-1], axis, up))
+    for _ in range((ways - 1) // 2):
+        later.append(lax.ppermute(later[-1], axis, down))
+    line = jnp.concatenate([*earlier[::-1], *later[1:]], axis=dim)
+    return jnp.roll(line, (lax.axis_index(axis) - ways // 2) * x.shape[dim], axis=dim)
 
 
 def two_words(x):
@@ -197,7 +210,7 @@
     units = jnp.square(
         jax.nn.relu(shares[:unit_count] * lax.rsqrt(sq_sum / D + EPS)[None, :])
     ).astype(BF16)
-    hidden_units = lax.all_gather(units, "kv", axis=0, tiled=True)
+    hidden_units = collect(units, "kv", 0)
     lowered = lax.dot_general(
         hidden_units, down_weight, (((0,), (0,)), ((), ())), preferred_element_type=F32
     ).astype(BF16)

time: 201 us -> 230 us (1.14)
  starting transfers between devices: 76.7 us -> 128 us
  waiting for transfers between devices: 55.3 us -> 32.5 us
    ppermute x0 -> x15, starting transfers between devices: none -> 49.3 us  [the longest x7 32.5 us: collect(): later.append(lax.ppermute(later[-1], axis, down))]
    all_to_all x0 -> x1, blocking collectives: none -> 36.9 us  [per_device(): arrived = lax.all_to_all(sent, 'kv', 0, 0, tiled=True)]
    all_gather x1 -> x0, blocking collectives: 27.8 us -> none  [per_device(): hidden_units = lax.all_gather(units, 'kv', axis=0, tiled=True)]
    all_to_all x2 -> x1, waiting for transfers between devices: 37.3 us -> 11.1 us  [per_device(): arrived = lax.all_to_all(sent, 'kv', 0, 0, tiled=True)]
    all_to_all x1, blocking collectives: 21.7 us -> 13.4 us  [per_device(): lowered = lax.all_to_all(lowered, ('dp', 'tp'), 0, 0, tiled=True)]
    ppermute x4, starting transfers between devices: 8.98 us -> 14.9 us  [from_partner(): return lax.ppermute(x, 'tp', [(i, (i + 1) % size) for i in range(size)])]
    all_to_all x2 -> x1, starting transfers between devices: 48.2 us -> 44.2 us  [per_device(): arrived = lax.all_to_all(sent, 'kv', 0, 0, tiled=True)]
    ppermute x0 -> x15, waiting for transfers between devices: none -> 3.54 us  [the longest x8 2.73 us: collect(): earlier.append(lax.ppermute(earlier[-1], axis, up))]
  transfers between devices with their start and end apart: 8 -> 22, of which waited for: 4 -> 5; matrix products, arithmetic and copies ran while one was open for 1% -> 1% of each run, Pallas kernels for 0% -> 0%
where the time goes in v1:
time: 230 us; the launch traced here: 228 us
  starting transfers between devices  128 us (56%)
  blocking collectives  50.3 us (22%)
  waiting for transfers between devices  32.5 us (14%)
  matrix products  6.95 us (3%)
  local copies, waits for them, and re-layouts  5.65 us (2%)
  other arithmetic  3.83 us (2%)
    all_to_all x1, starting transfers between devices, per_device(): arrived = lax.all_to_all(sent, 'kv', 0, 0, tiled=True)  44.2 us
    all_to_all x1, blocking collectives, per_device(): arrived = lax.all_to_all(sent, 'kv', 0, 0, tiled=True)  36.9 us
    ppermute x7, starting transfers between devices, collect(): later.append(lax.ppermute(later[-1], axis, down))  32.5 us
    all_to_all x2, starting transfers between devices, to_everyone(): lax.all_to_all(jnp.broadcast_to(shard[None], (size, *shard.shape)), axes,...  19.5 us
    all_to_all x2, waiting for transfers between devices, to_everyone(): lax.all_to_all(jnp.broadcast_to(shard[None], (size, *shard.shape)), axes,...  17.9 us
    ppermute x8, starting transfers between devices, collect(): earlier.append(lax.ppermute(earlier[-1], axis, up))  16.8 us
    ppermute x4, starting transfers between devices, from_partner(): return lax.ppermute(x, 'tp', [(i, (i + 1) % size) for i in range(size)])  14.9 us
    all_to_all x1, blocking collectives, per_device(): lowered = lax.all_to_all(lowered, ('dp', 'tp'), 0, 0, tiled=True)  13.4 us
  transfers between devices with their start and end apart: 22, of which 5 were waited for; matrix products, arithmetic and copies ran while one was open for 1% of the time, Pallas kernels for 0%

profile of v1, /device:TPU:65, one launch (start us, length us, event | category | flops | bytes accessed | tf_op | source)
XLA Modules:
  0.0 228.3 jit_solution(8083758147317969679)
XLA Ops:
  6.7 44.2 %all-to-all-start = ((bf16[16,2,3200]{2,1,0:T(2,128)(2,1)}), bf16[16,2,3200]{2,1,0:T(2,128)(2,1)S(1)}, u32[]{:S(2)}, u32[]{:S(2)}) async-start(bf16[16,2,3200]{2,1,0:T(2,128)(2,1)} %concatenate.58), calls=%async_computation | async-start | bytes 409600 | tf_op jit(solution)/shard_map/all_to_all | solution.py:114
  52.0 11.1 %all-to-all-done = bf16[16,2,3200]{2,1,0:T(2,128)(2,1)S(1)} async-done(((bf16[16,2,3200]{2,1,0:T(2,128)(2,1)}), bf16[16,2,3200]{2,1,0:T(2,128)(2,1)S(1)}, u32[]{:S(2)}, u32[]{:S(2)}) %all-to-all-start) | async-done | bytes 204832 | tf_op jit(solution)/shard_map/all_to_all | solution.py:114
  68.1 10.6 %all-to-all-start.1 = ((bf16[32,2,1152]{2,1,0:T(2,128)(2,1)}), bf16[32,2,1152]{2,1,0:T(2,128)(2,1)S(1)}, u32[]{:S(2)}, u32[]{:S(2)}) async-start(bf16[32,2,1152]{2,1,0:T(2,128)(2,1)} %broadcast_in_dim.23), calls=%async_computation.1 | async-start | bytes 294912 | tf_op jit(solution)/shard_map/all_to_all | solution.py:37
  78.8 2.6 %collective-permute-start = (bf16[1024,128]{1,0:T(8,128)(2,1)S(1)}, bf16[1024,128]{1,0:T(8,128)(2,1)S(1)}, u32[]{:S(2)}, u32[]{:S(2)}) collective-permute-start(bf16[1024,128]{1,0:T(8,128)(2,1)S(1)} %get-tuple-element.16), channel_id=1, source_target_pairs={{0,1},{1,0},{2,3},{3,2},{4,5},{5,4},{6,7},{7,6},{8,9},{9,8},{10,11... | collective-permute-start | bytes 786440 | tf_op jit(solution)/shard_map/ppermute | solution.py:44
  81.4 13.6 %all-to-all-done.1 = bf16[32,2,1152]{2,1,0:T(2,128)(2,1)S(1)} async-done(((bf16[32,2,1152]{2,1,0:T(2,128)(2,1)}), bf16[32,2,1152]{2,1,0:T(2,128)(2,1)S(1)}, u32[]{:S(2)}, u32[]{:S(2)}) %all-to-all-start.1) | async-done | bytes 147488 | tf_op jit(solution)/shard_map/all_to_all | solution.py:37
  96.8 8.9 %all-to-all-start.2 = ((bf16[16,32,128]{2,1,0:T(8,128)(2,1)}), bf16[16,32,128]{2,1,0:T(8,128)(2,1)S(1)}, u32[]{:S(2)}, u32[]{:S(2)}) async-start(bf16[16,32,128]{2,1,0:T(8,128)(2,1)} %broadcast_in_dim.24), calls=%async_computation.2 | async-start | bytes 262144 | tf_op jit(solution)/shard_map/all_to_all | solution.py:37
  105.8 2.2 collective-permute-start.2
  108.1 2.1 collective-permute-start.1
  110.3 4.3 %all-to-all-done.2 = bf16[16,32,128]{2,1,0:T(8,128)(2,1)S(1)} async-done(((bf16[16,32,128]{2,1,0:T(8,128)(2,1)}), bf16[16,32,128]{2,1,0:T(8,128)(2,1)S(1)}, u32[]{:S(2)}, u32[]{:S(2)}) %all-to-all-start.2) | async-done | bytes 131104 | tf_op jit(solution)/shard_map/all_to_all | solution.py:37
  115.3 36.9 %all_to_all.25 = bf16[16,72,256]{2,1,0:T(8,128)(2,1)S(1)} all-to-all(bf16[16,72,256]{2,1,0:T(8,128)(2,1)S(1)} %pad_maximum_fusion), channel_id=1, replica_groups=mesh['grp'=2,'dp'=8,'kv'=16,'tp'=2] {'kv'}, dimensions={0} | all-to-all | bytes 1179648 | tf_op jit(solution)/shard_map/all_to_all | solution.py:206
  152.3 3.2 %collective-permute-start.3 = (bf16[64,256]{1,0:T(8,128)(2,1)S(1)}, bf16[64,256]{1,0:T(8,128)(2,1)S(1)}, u32[]{:S(2)}, u32[]{:S(2)}) collective-permute-start(bf16[64,256]{1,0:T(8,128)(2,1)S(1)} %fusion.25), channel_id=1, source_target_pairs={{0,2},{2,4},{4,6},{6,8},{8,10},{10,12},{12,14},{14,16},{16,18},{18... | collective-permute-start | bytes 98312 | tf_op jit(solution)/shard_map/ppermute | solution.py:23
  155.5 2.7 %collective-permute-done.3 = bf16[64,256]{1,0:T(8,128)(2,1)S(1)} collective-permute-done((bf16[64,256]{1,0:T(8,128)(2,1)S(1)}, bf16[64,256]{1,0:T(8,128)(2,1)S(1)}, u32[]{:S(2)}, u32[]{:S(2)}) %collective-permute-start.3) | collective-permute-done | bytes 32800 | tf_op jit(solution)/shard_map/ppermute | solution.py:23
  158.2 2.0 collective-permute-start.4
  160.2 4.6 %collective-permute-start.11 = (bf16[64,256]{1,0:T(8,128)(2,1)S(1)}, bf16[64,256]{1,0:T(8,128)(2,1)S(1)}, u32[]{:S(2)}, u32[]{:S(2)}) collective-permute-start(bf16[64,256]{1,0:T(8,128)(2,1)S(1)} %fusion.25), channel_id=1, source_target_pairs={{0,30},{2,0},{4,2},{6,4},{8,6},{10,8},{12,10},{14,12},{16,14},{18,... | collective-permute-start | bytes 98312 | tf_op jit(solution)/shard_map/ppermute | solution.py:25
  164.8 2.0 collective-permute-start.5
  166.8 4.6 %collective-permute-start.12 = (bf16[64,256]{1,0:T(8,128)(2,1)S(1)}, bf16[64,256]{1,0:T(8,128)(2,1)S(1)}, u32[]{:S(2)}, u32[]{:S(2)}) collective-permute-start(bf16[64,256]{1,0:T(8,128)(2,1)S(1)} %collective-permute-done.11), channel_id=1, source_target_pairs={{0,30},{2,0},{4,2},{6,4},{8,6},{10,8},{12,10},{14,12},{16,14},{18,... | collective-permute-start | bytes 98312 | tf_op jit(solution)/shard_map/ppermute | solution.py:25
  171.4 2.0 collective-permute-start.6
  173.4 4.6 %collective-permute-start.13 = (bf16[64,256]{1,0:T(8,128)(2,1)S(1)}, bf16[64,256]{1,0:T(8,128)(2,1)S(1)}, u32[]{:S(2)}, u32[]{:S(2)}) collective-permute-start(bf16[64,256]{1,0:T(8,128)(2,1)S(1)} %collective-permute-done.12), channel_id=1, source_target_pairs={{0,30},{2,0},{4,2},{6,4},{8,6},{10,8},{12,10},{14,12},{16,14},{18,... | collective-permute-start | bytes 98312 | tf_op jit(solution)/shard_map/ppermute | solution.py:25
  180.0 4.6 %collective-permute-start.14 = (bf16[64,256]{1,0:T(8,128)(2,1)S(1)}, bf16[64,256]{1,0:T(8,128)(2,1)S(1)}, u32[]{:S(2)}, u32[]{:S(2)}) collective-permute-start(bf16[64,256]{1,0:T(8,128)(2,1)S(1)} %collective-permute-done.13), channel_id=1, source_target_pairs={{0,30},{2,0},{4,2},{6,4},{8,6},{10,8},{12,10},{14,12},{16,14},{18,... | collective-permute-start | bytes 98312 | tf_op jit(solution)/shard_map/ppermute | solution.py:25
  186.5 4.6 %collective-permute-start.15 = (bf16[64,256]{1,0:T(8,128)(2,1)S(1)}, bf16[64,256]{1,0:T(8,128)(2,1)S(1)}, u32[]{:S(2)}, u32[]{:S(2)}) collective-permute-start(bf16[64,256]{1,0:T(8,128)(2,1)S(1)} %collective-permute-done.14), channel_id=1, source_target_pairs={{0,30},{2,0},{4,2},{6,4},{8,6},{10,8},{12,10},{14,12},{16,14},{18,... | collective-permute-start | bytes 98312 | tf_op jit(solution)/shard_map/ppermute | solution.py:25
  193.1 4.6 %collective-permute-start.16 = (bf16[64,256]{1,0:T(8,128)(2,1)S(1)}, bf16[64,256]{1,0:T(8,128)(2,1)S(1)}, u32[]{:S(2)}, u32[]{:S(2)}) collective-permute-start(bf16[64,256]{1,0:T(8,128)(2,1)S(1)} %collective-permute-done.15), channel_id=1, source_target_pairs={{0,30},{2,0},{4,2},{6,4},{8,6},{10,8},{12,10},{14,12},{16,14},{18,... | collective-permute-start | bytes 98312 | tf_op jit(solution)/shard_map/ppermute | solution.py:25
  199.8 7.9 %collective-permute-start.18 = (bf16[1024,128]{1,0:T(8,128)(2,1)S(1)}, bf16[1024,128]{1,0:T(8,128)(2,1)S(1)}, u32[]{:S(2)}, u32[]{:S(2)}) collective-permute-start(bf16[1024,128]{1,0:T(8,128)(2,1)S(1)} %get-tuple-element.18), channel_id=1, source_target_pairs={{0,1},{1,0},{2,3},{3,2},{4,5},{5,4},{6,7},{7,6},{8,9},{9,8},{10,11... | collective-permute-start | bytes 786440 | tf_op jit(solution)/shard_map/ppermute | solution.py:44
  207.7 4.9 %collective-permute-start.17 = (bf16[64,256]{1,0:T(8,128)(2,1)S(1)}, bf16[64,256]{1,0:T(8,128)(2,1)S(1)}, u32[]{:S(2)}, u32[]{:S(2)}) collective-permute-start(bf16[64,256]{1,0:T(8,128)(2,1)S(1)} %collective-permute-done.16), channel_id=1, source_target_pairs={{0,30},{2,0},{4,2},{6,4},{8,6},{10,8},{12,10},{14,12},{16,14},{18,... | collective-permute-start | bytes 98312 | tf_op jit(solution)/shard_map/ppermute | solution.py:25
  214.3 13.4 %all_to_all.26 = bf16[16,32,128]{2,1,0:T(8,128)(2,1)S(1)} all-to-all(bf16[16,32,128]{2,1,0:T(8,128)(2,1)S(1)} %bitcast.104), channel_id=1, replica_groups=mesh['grp'=2,'dp'=8,'kv'=16,'tp'=2] {'dp','tp'}, dimensions={0} | all-to-all | bytes 262144 | tf_op jit(solution)/shard_map/all_to_all | solution.py:219
  (188 shorter events, 25.1 us)
Async XLA Ops:
  0.0 65.0 %copy-start = (f32[2,16,64,128]{3,2,1,0:T(8,128)S(1)}, f32[2,16,64,128]{3,2,1,0:T(8,128)}, u32[]{:S(2)}) copy-start(f32[2,16,64,128]{3,2,1,0:T(8,128)} %param.44) | copy-start | bytes 3145732
  6.7 56.4 %all-to-all-start = ((bf16[16,2,3200]{2,1,0:T(2,128)(2,1)}), bf16[16,2,3200]{2,1,0:T(2,128)(2,1)S(1)}, u32[]{:S(2)}, u32[]{:S(2)}) async-start(bf16[16,2,3200]{2,1,0:T(2,128)(2,1)} %concatenate.58), calls=%async_computation | async-start | bytes 409600 | tf_op jit(solution)/shard_map/all_to_all | solution.py:114
  68.1 26.9 %all-to-all-start.1 = ((bf16[32,2,1152]{2,1,0:T(2,128)(2,1)}), bf16[32,2,1152]{2,1,0:T(2,128)(2,1)S(1)}, u32[]{:S(2)}, u32[]{:S(2)}) async-start(bf16[32,2,1152]{2,1,0:T(2,128)(2,1)} %broadcast_in_dim.23), calls=%async_computation.1 | async-start | bytes 294912 | tf_op jit(solution)/shard_map/all_to_all | solution.py:37
  78.8 17.2 %collective-permute-start = (bf16[1024,128]{1,0:T(8,128)(2,1)S(1)}, bf16[1024,128]{1,0:T(8,128)(2,1)S(1)}, u32[]{:S(2)}, u32[]{:S(2)}) collective-permute-start(bf16[1024,128]{1,0:T(8,128)(2,1)S(1)} %get-tuple-element.16), channel_id=1, source_target_pairs={{0,1},{1,0},{2,3},{3,2},{4,5},{5,4},{6,7},{7,6},{8,9},{9,8},{10,11... | collective-permute-start | bytes 786440 | tf_op jit(solution)/shard_map/ppermute | solution.py:44
  96.8 17.8 %all-to-all-start.2 = ((bf16[16,32,128]{2,1,0:T(8,128)(2,1)}), bf16[16,32,128]{2,1,0:T(8,128)(2,1)S(1)}, u32[]{:S(2)}, u32[]{:S(2)}) async-start(bf16[16,32,128]{2,1,0:T(8,128)(2,1)} %broadcast_in_dim.24), calls=%async_computation.2 | async-start | bytes 262144 | tf_op jit(solution)/shard_map/all_to_all | solution.py:37
  105.8 4.6 %collective-permute-start.2 = (f32[128]{0:T(128)S(1)}, f32[128]{0:T(128)S(1)}, u32[]{:S(2)}, u32[]{:S(2)}) collective-permute-start(f32[128]{0:T(128)S(1)} %copy-done.19), channel_id=1, source_target_pairs={{0,1},{1,0},{2,3},{3,2},{4,5},{5,4},{6,7},{7,6},{8,9},{9,8},{10,11... | collective-permute-start | bytes 1544 | tf_op jit(solution)/shard_map/ppermute | solution.py:44
  108.1 6.8 %collective-permute-start.1 = (bf16[128,1024]{1,0:T(8,128)(2,1)S(1)}, bf16[128,1024]{1,0:T(8,128)(2,1)S(1)}, u32[]{:S(2)}, u32[]{:S(2)}) collective-permute-start(bf16[128,1024]{1,0:T(8,128)(2,1)S(1)} %get-tuple-element.14), channel_id=1, source_target_pairs={{0,1},{1,0},{2,3},{3,2},{4,5},{5,4},{6,7},{7,6},{8,9},{9,8},{10,11... | collective-permute-start | bytes 786440 | tf_op jit(solution)/shard_map/ppermute | solution.py:44
  115.3 84.4 %copy-start.4 = (bf16[2048,128]{1,0:T(8,128)(2,1)S(1)}, bf16[2048,128]{1,0:T(8,128)(2,1)}, u32[]{:S(2)}) copy-start(bf16[2048,128]{1,0:T(8,128)(2,1)} %param.49) | copy-start | bytes 1572868
  152.3 5.9 %collective-permute-start.3 = (bf16[64,256]{1,0:T(8,128)(2,1)S(1)}, bf16[64,256]{1,0:T(8,128)(2,1)S(1)}, u32[]{:S(2)}, u32[]{:S(2)}) collective-permute-start(bf16[64,256]{1,0:T(8,128)(2,1)S(1)} %fusion.25), channel_id=1, source_target_pairs={{0,2},{2,4},{4,6},{6,8},{8,10},{10,12},{12,14},{14,16},{16,18},{18... | collective-permute-start | bytes 98312 | tf_op jit(solution)/shard_map/ppermute | solution.py:23
  158.2 6.6 %collective-permute-start.4 = (bf16[64,256]{1,0:T(8,128)(2,1)S(1)}, bf16[64,256]{1,0:T(8,128)(2,1)S(1)}, u32[]{:S(2)}, u32[]{:S(2)}) collective-permute-start(bf16[64,256]{1,0:T(8,128)(2,1)S(1)} %collective-permute-done.3), channel_id=1, source_target_pairs={{0,2},{2,4},{4,6},{6,8},{8,10},{10,12},{12,14},{14,16},{16,18},{18... | collective-permute-start | bytes 98312 | tf_op jit(solution)/shard_map/ppermute | solution.py:23
  160.2 6.6 %collective-permute-start.11 = (bf16[64,256]{1,0:T(8,128)(2,1)S(1)}, bf16[64,256]{1,0:T(8,128)(2,1)S(1)}, u32[]{:S(2)}, u32[]{:S(2)}) collective-permute-start(bf16[64,256]{1,0:T(8,128)(2,1)S(1)} %fusion.25), channel_id=1, source_target_pairs={{0,30},{2,0},{4,2},{6,4},{8,6},{10,8},{12,10},{14,12},{16,14},{18,... | collective-permute-start | bytes 98312 | tf_op jit(solution)/shard_map/ppermute | solution.py:25
  164.8 6.6 %collective-permute-start.5 = (bf16[64,256]{1,0:T(8,128)(2,1)S(1)}, bf16[64,256]{1,0:T(8,128)(2,1)S(1)}, u32[]{:S(2)}, u32[]{:S(2)}) collective-permute-start(bf16[64,256]{1,0:T(8,128)(2,1)S(1)} %collective-permute-done.4), channel_id=1, source_target_pairs={{0,2},{2,4},{4,6},{6,8},{8,10},{10,12},{12,14},{14,16},{16,18},{18... | collective-permute-start | bytes 98312 | tf_op jit(solution)/shard_map/ppermute | solution.py:23
  166.8 6.6 %collective-permute-start.12 = (bf16[64,256]{1,0:T(8,128)(2,1)S(1)}, bf16[64,256]{1,0:T(8,128)(2,1)S(1)}, u32[]{:S(2)}, u32[]{:S(2)}) collective-permute-start(bf16[64,256]{1,0:T(8,128)(2,1)S(1)} %collective-permute-done.11), channel_id=1, source_target_pairs={{0,30},{2,0},{4,2},{6,4},{8,6},{10,8},{12,10},{14,12},{16,14},{18,... | collective-permute-start | bytes 98312 | tf_op jit(solution)/shard_map/ppermute | solution.py:25
  171.4 6.6 %collective-permute-start.6 = (bf16[64,256]{1,0:T(8,128)(2,1)S(1)}, bf16[64,256]{1,0:T(8,128)(2,1)S(1)}, u32[]{:S(2)}, u32[]{:S(2)}) collective-permute-start(bf16[64,256]{1,0:T(8,128)(2,1)S(1)} %collective-permute-done.5), channel_id=1, source_target_pairs={{0,2},{2,4},{4,6},{6,8},{8,10},{10,12},{12,14},{14,16},{16,18},{18... | collective-permute-start | bytes 98312 | tf_op jit(solution)/shard_map/ppermute | solution.py:23
  173.4 6.6 %collective-permute-start.13 = (bf16[64,256]{1,0:T(8,128)(2,1)S(1)}, bf16[64,256]{1,0:T(8,128)(2,1)S(1)}, u32[]{:S(2)}, u32[]{:S(2)}) collective-permute-start(bf16[64,256]{1,0:T(8,128)(2,1)S(1)} %collective-permute-done.12), channel_id=1, source_target_pairs={{0,30},{2,0},{4,2},{6,4},{8,6},{10,8},{12,10},{14,12},{16,14},{18,... | collective-permute-start | bytes 98312 | tf_op jit(solution)/shard_map/ppermute | solution.py:25
  178.0 6.6 %collective-permute-start.7 = (bf16[64,256]{1,0:T(8,128)(2,1)S(1)}, bf16[64,256]{1,0:T(8,128)(2,1)S(1)}, u32[]{:S(2)}, u32[]{:S(2)}) collective-permute-start(bf16[64,256]{1,0:T(8,128)(2,1)S(1)} %collective-permute-done.6), channel_id=1, source_target_pairs={{0,2},{2,4},{4,6},{6,8},{8,10},{10,12},{12,14},{14,16},{16,18},{18... | collective-permute-start | bytes 98312 | tf_op jit(solution)/shard_map/ppermute | solution.py:23
  180.0 6.6 %collective-permute-start.14 = (bf16[64,256]{1,0:T(8,128)(2,1)S(1)}, bf16[64,256]{1,0:T(8,128)(2,1)S(1)}, u32[]{:S(2)}, u32[]{:S(2)}) collective-permute-start(bf16[64,256]{1,0:T(8,128)(2,1)S(1)} %collective-permute-done.13), channel_id=1, source_target_pairs={{0,30},{2,0},{4,2},{6,4},{8,6},{10,8},{12,10},{14,12},{16,14},{18,... | collective-permute-start | bytes 98312 | tf_op jit(solution)/shard_map/ppermute | solution.py:25
  184.6 6.6 %collective-permute-start.8 = (bf16[64,256]{1,0:T(8,128)(2,1)S(1)}, bf16[64,256]{1,0:T(8,128)(2,1)S(1)}, u32[]{:S(2)}, u32[]{:S(2)}) collective-permute-start(bf16[64,256]{1,0:T(8,128)(2,1)S(1)} %collective-permute-done.7), channel_id=1, source_target_pairs={{0,2},{2,4},{4,6},{6,8},{8,10},{10,12},{12,14},{14,16},{16,18},{18... | collective-permute-start | bytes 98312 | tf_op jit(solution)/shard_map/ppermute | solution.py:23
  186.5 6.6 %collective-permute-start.15 = (bf16[64,256]{1,0:T(8,128)(2,1)S(1)}, bf16[64,256]{1,0:T(8,128)(2,1)S(1)}, u32[]{:S(2)}, u32[]{:S(2)}) collective-permute-start(bf16[64,256]{1,0:T(8,128)(2,1)S(1)} %collective-permute-done.14), channel_id=1, source_target_pairs={{0,30},{2,0},{4,2},{6,4},{8,6},{10,8},{12,10},{14,12},{16,14},{18,... | collective-permute-start | bytes 98312 | tf_op jit(solution)/shard_map/ppermute | solution.py:25
  191.2 6.6 %collective-permute-start.9 = (bf16[64,256]{1,0:T(8,128)(2,1)S(1)}, bf16[64,256]{1,0:T(8,128)(2,1)S(1)}, u32[]{:S(2)}, u32[]{:S(2)}) collective-permute-start(bf16[64,256]{1,0:T(8,128)(2,1)S(1)} %collective-permute-done.8), channel_id=1, source_target_pairs={{0,2},{2,4},{4,6},{6,8},{8,10},{10,12},{12,14},{14,16},{16,18},{18... | collective-permute-start | bytes 98312 | tf_op jit(solution)/shard_map/ppermute | solution.py:23
  193.1 14.6 %collective-permute-start.16 = (bf16[64,256]{1,0:T(8,128)(2,1)S(1)}, bf16[64,256]{1,0:T(8,128)(2,1)S(1)}, u32[]{:S(2)}, u32[]{:S(2)}) collective-permute-start(bf16[64,256]{1,0:T(8,128)(2,1)S(1)} %collective-permute-done.15), channel_id=1, source_target_pairs={{0,30},{2,0},{4,2},{6,4},{8,6},{10,8},{12,10},{14,12},{16,14},{18,... | collective-permute-start | bytes 98312 | tf_op jit(solution)/shard_map/ppermute | solution.py:25
  197.8 14.9 %collective-permute-start.10 = (bf16[64,256]{1,0:T(8,128)(2,1)S(1)}, bf16[64,256]{1,0:T(8,128)(2,1)S(1)}, u32[]{:S(2)}, u32[]{:S(2)}) collective-permute-start(bf16[64,256]{1,0:T(8,128)(2,1)S(1)} %collective-permute-done.9), channel_id=1, source_target_pairs={{0,2},{2,4},{4,6},{6,8},{8,10},{10,12},{12,14},{14,16},{16,18},{18... | collective-permute-start | bytes 98312 | tf_op jit(solution)/shard_map/ppermute | solution.py:23
  199.8 14.1 %collective-permute-start.18 = (bf16[1024,128]{1,0:T(8,128)(2,1)S(1)}, bf16[1024,128]{1,0:T(8,128)(2,1)S(1)}, u32[]{:S(2)}, u32[]{:S(2)}) collective-permute-start(bf16[1024,128]{1,0:T(8,128)(2,1)S(1)} %get-tuple-element.18), channel_id=1, source_target_pairs={{0,1},{1,0},{2,3},{3,2},{4,5},{5,4},{6,7},{7,6},{8,9},{9,8},{10,11... | collective-permute-start | bytes 786440 | tf_op jit(solution)/shard_map/ppermute | solution.py:44
  207.7 5.9 %collective-permute-start.17 = (bf16[64,256]{1,0:T(8,128)(2,1)S(1)}, bf16[64,256]{1,0:T(8,128)(2,1)S(1)}, u32[]{:S(2)}, u32[]{:S(2)}) collective-permute-start(bf16[64,256]{1,0:T(8,128)(2,1)S(1)} %collective-permute-done.16), channel_id=1, source_target_pairs={{0,30},{2,0},{4,2},{6,4},{8,6},{10,8},{12,10},{14,12},{16,14},{18,... | collective-permute-start | bytes 98312 | tf_op jit(solution)/shard_map/ppermute | solution.py:25
  (20 other events, 343.4 us)
